TPU v7x, 32 devices: a whole 2x2x4 slice. The times are simulated.
32 devices in a mesh: ep: 4 (over y, x), tp: 8 (over z, core).
Axes of the slice: x: 2, y: 2, z: 4, core: 2. Of those that a mesh axis runs over, the one named last changes fastest.
Arguments:
- tokens: bfloat16 [512, 2048], P('ep'), may hold values from -6 to 6
- conv_state: bfloat16 [512, 3, 2048], P('ep', None, 'tp'), may hold values from -6 to 6
- rec_state: float32 [512, 2048], P('ep', 'tp'), may hold values from -6 to 6
- gate_proj: bfloat16 [2048, 2048], P(None, 'tp'), may hold values from -0.125 to 0.125
- input_proj: bfloat16 [2048, 2048], P(None, 'tp'), may hold values from -0.125 to 0.125
- conv_taps: bfloat16 [4, 2048], P(None, 'tp'), may hold values from -3 to 3
- decay_blocks: bfloat16 [16, 128, 128], P('tp'), may hold values from -0.5 to 0.5
- input_blocks: bfloat16 [16, 128, 128], P('tp'), may hold values from -0.5 to 0.5
- decay_param: float32 [2048], P('tp'), may hold values from 0 to 6
- out_proj: bfloat16 [2048, 2048], P('tp'), may hold values from -0.125 to 0.125
- first_gain: float32 [2048], replicated, may hold values from 0.1 to 1.9
- expert_gate: bfloat16 [4, 2048, 7168], P('ep', None, 'tp'), may hold values from -0.125 to 0.125
- expert_up: bfloat16 [4, 2048, 7168], P('ep', None, 'tp'), may hold values from -0.125 to 0.125
- expert_down: bfloat16 [4, 7168, 2048], P('ep', 'tp'), may hold values from -0.0625 to 0.0625
- routing: int32 [512, 2], P('ep'), may hold values from 0 to 3, all different within a row; in each aligned block of 128 rows (0 to 127, 128 to 255, ...) at most 128 rows name the same one
- route_weight: float32 [512, 2], P('ep'), may hold values from 0.1 to 1
- dense_gate: bfloat16 [2048, 2048], P(None, 'tp'), may hold values from -0.125 to 0.125
- dense_up: bfloat16 [2048, 2048], P(None, 'tp'), may hold values from -0.125 to 0.125
- dense_down: bfloat16 [2048, 2048], P('tp'), may hold values from -0.125 to 0.125
- mix_weight: bfloat16 [2048], replicated, may hold values from -0.125 to 0.125
- second_gain: float32 [2048], P('tp'), may hold values from 0.1 to 1.9
Outputs:
- layer_out: bfloat16 [512, 2048], P('ep', 'tp')
- new_state: float32 [512, 2048], P('ep', 'tp')
- new_conv: bfloat16 [512, 3, 2048], P('ep', None, 'tp')
Inputs may be any that keep to these rules, and one draw needn't show every extreme that they name: `routing`: each row names 2 different experts; in each aligned block of 128 rows (the rows of one index of ep) no expert is named by more than 128 rows, a bound that some expert reaches in some block.
All inputs are finite; a program needn't handle non-finite values.
Results may differ from a plain program's by a relative error of at most 0.013.
Values may be sent and summed in bfloat16 or wider, within the bound.
A program may use at most 64 MiB of HBM per device.

v0:
```python
import jax
import jax.numpy as jnp
from jax import lax
from jax.sharding import PartitionSpec as P

D = 2048
TOPK = 2
ALPHA = 8.0**0.25
RATE_SCALE = 8.0
NORM_EPS = 1e-05


def norm_rows(values, gain_vec):
    centre = values - jnp.mean(values, axis=-1, keepdims=True)
    spread = jnp.mean(centre * centre, axis=-1, keepdims=True)
    return centre * lax.rsqrt(spread + NORM_EPS) * gain_vec


def on_device(
    tokens,
    conv_state,
    rec_state,
    gate_proj,
    input_proj,
    conv_taps,
    decay_blocks,
    input_blocks,
    decay_param,
    out_proj,
    first_gain,
    expert_gate,
    expert_up,
    expert_down,
    routing,
    route_weight,
    dense_gate,
    dense_up,
    dense_down,
    mix_weight,
    second_gain,
):
    count_rows = tokens.shape[0]
    gated = jnp.dot(tokens, gate_proj, preferred_element_type=jnp.float32).astype(jnp.bfloat16)
    inputs = jnp.dot(tokens, input_proj, preferred_element_type=jnp.float32).astype(jnp.bfloat16)
    window = jnp.concatenate([conv_state, inputs[:, None, :]], axis=1)
    convolved = jnp.sum(
        window.astype(jnp.float32) * conv_taps.astype(jnp.float32)[None], axis=1
    ).astype(jnp.bfloat16)
    local_heads = decay_blocks.shape[0]
    heads_view = convolved.reshape(count_rows, local_heads, -1)
    recur_gate = jax.nn.sigmoid(
        jnp.einsum("bhi,hij->bhj", heads_view, decay_blocks, preferred_element_type=jnp.float32)
    ).reshape(count_rows, -1)
    input_gate = jax.nn.sigmoid(
        jnp.einsum("bhi,hij->bhj", heads_view, input_blocks, preferred_element_type=jnp.float32)
    ).reshape(count_rows, -1)
    log_decay = -RATE_SCALE * recur_gate * jax.nn.softplus(-decay_param)
    new_state = jnp.exp(log_decay) * rec_state + jnp.sqrt(
        -jnp.expm1(2.0 * log_decay)
    ) * input_gate * convolved.astype(jnp.float32)
    mixed_rows = (new_state * jax.nn.gelu(gated.astype(jnp.float32), approximate=True)).astype(
        jnp.bfloat16
    )
    partial_mix = jnp.dot(mixed_rows, out_proj, preferred_element_type=jnp.float32)
    mixed = lax.psum(partial_mix.astype(jnp.bfloat16), "tp").astype(jnp.float32)
    normed = norm_rows(ALPHA * tokens.astype(jnp.float32) + mixed, first_gain).astype(jnp.bfloat16)
    tp_index = lax.axis_index("tp")
    tp_count = lax.axis_size("tp")
    own_width = D // tp_count
    own_normed = lax.dynamic_slice_in_dim(normed, tp_index * own_width, own_width, 1)
    local_experts = expert_gate.shape[0]
    ep_count = lax.axis_size("ep")
    experts = local_experts * ep_count
    capacity = max(2, 2 * count_rows * TOPK // experts)
    flat_routes = routing.reshape(-1)
    labels = jnp.arange(experts, dtype=jnp.int32)
    onehot = (flat_routes[:, None] == labels[None, :]).astype(jnp.int32)
    earlier = jnp.cumsum(onehot, axis=0) - onehot
    slot_index = jnp.sum(earlier * onehot, axis=1)
    target = flat_routes * capacity + slot_index
    placed = (target[:, None] == jnp.arange(experts * capacity, dtype=jnp.int32)[None, :]).astype(
        jnp.bfloat16
    )
    token_slots = jnp.sum(placed.reshape(count_rows, TOPK, experts * capacity), axis=1)
    dispatch = jnp.dot(token_slots.T, normed, preferred_element_type=jnp.float32).astype(
        jnp.bfloat16
    )
    arrived = lax.all_to_all(
        dispatch.reshape(experts, capacity, D), "ep", split_axis=0, concat_axis=1, tiled=True
    )
    gate_val = jnp.einsum("erd,edf->erf", arrived, expert_gate, preferred_element_type=jnp.float32)
    up_val = jnp.einsum("erd,edf->erf", arrived, expert_up, preferred_element_type=jnp.float32)
    hidden = (jax.nn.silu(gate_val) * up_val).astype(jnp.bfloat16)
    partial_out = jnp.einsum(
        "erf,efd->erd", hidden, expert_down, preferred_element_type=jnp.float32
    )
    reduced = lax.psum_scatter(
        partial_out.astype(jnp.bfloat16), "tp", scatter_dimension=2, tiled=True
    )
    returned = lax.all_to_all(reduced, "ep", split_axis=1, concat_axis=0, tiled=True)
    returned = returned.reshape(experts * capacity, own_width)
    picked = jnp.dot(placed, returned, preferred_element_type=jnp.float32).reshape(
        count_rows, TOPK, own_width
    )
    routed_sum = jnp.sum(route_weight[:, :, None] * picked, axis=1)
    dense_g = jnp.dot(normed, dense_gate, preferred_element_type=jnp.float32)
    dense_u = jnp.dot(normed, dense_up, preferred_element_type=jnp.float32)
    dense_hidden = (jax.nn.silu(dense_g) * dense_u).astype(jnp.bfloat16)
    dense_part = jnp.dot(dense_hidden, dense_down, preferred_element_type=jnp.float32)
    dense_out = lax.psum_scatter(
        dense_part.astype(jnp.bfloat16), "tp", scatter_dimension=1, tiled=True
    ).astype(jnp.float32)
    mix = jax.nn.sigmoid(jnp.dot(normed, mix_weight, preferred_element_type=jnp.float32))
    combined = ALPHA * own_normed.astype(jnp.float32) + routed_sum + mix[:, None] * dense_out
    row_total, row_square = lax.psum(
        (jnp.sum(combined, axis=1), jnp.sum(combined * combined, axis=1)), "tp"
    )
    row_mean = row_total / D
    row_var = row_square / D - row_mean * row_mean
    layer_out = (
        (combined - row_mean[:, None]) * lax.rsqrt(row_var[:, None] + NORM_EPS) * second_gain
    ).astype(jnp.bfloat16)
    return (layer_out, new_state, window[:, 1:])


def solution(mesh):
    return jax.shard_map(
        on_device,
        mesh=mesh,
        in_specs=(
            P("ep", None),
            P("ep", None, "tp"),
            P("ep", "tp"),
            P(None, "tp"),
            P(None, "tp"),
            P(None, "tp"),
            P("tp", None, None),
            P("tp", None, None),
            P("tp"),
            P("tp", None),
            P(),
            P("ep", None, "tp"),
            P("ep", None, "tp"),
            P("ep", "tp", None),
            P("ep", None),
            P("ep", None),
            P(None, "tp"),
            P(None, "tp"),
            P("tp", None),
            P(),
            P("tp"),
        ),
        out_specs=(P("ep", "tp"), P("ep", "tp"), P("ep", None, "tp")),
        check_vma=False,
    )
```

profile of v0, /device:TPU:0, one launch (start us, length us, event | category | flops | bytes accessed | tf_op | source)
XLA Modules:
  0.0 208.7 jit_solution(3627572307212594813)
XLA Ops:
  7.2 0.0 copy-start
  7.2 0.0 copy-start.15
  7.2 0.0 copy-start.13
  7.2 0.0 copy-start.8
  7.2 0.0 all-reduce.3.cloned.1.call-start
  7.3 0.8 convert_element_type.84
  8.0 1.8 fusion.23
  9.8 1.0 multiply_reduce_fusion.1
  10.8 1.1 fusion.20
  11.9 0.1 copy.91
  12.0 0.0 copy-done.15
  12.0 0.2 fusion.17
  12.3 0.1 copy.94
  12.4 0.0 copy-done.13
  12.4 0.0 copy-start.10
  12.4 0.1 multiply_add_fusion.1
  12.6 0.0 copy-start.7
  12.6 1.6 convolution_convert_fusion.2
  14.2 0.0 all-reduce.3.cloned.1.call-update
  14.2 0.0 reduce-scatter.3.cloned.1.call-start
  14.3 0.1 copy.95
  14.4 0.1 eq.65
  14.5 0.1 eq.61
  14.7 1.2 reduce-window.6
  15.9 0.1 slice.12
  16.0 0.1 copy.97
  16.1 0.1 copy.98
  16.2 0.1 add_bitcast_fusion
  16.3 0.1 reduce_sum.81
  16.5 0.1 copy.99
  16.6 0.1 fusion.34
  16.7 56.9 %all-reduce.3.cloned.1.call-done = bf16[128,2048]{1,0:T(8,128)(2,1)} async-done(((bf16[128,2048]{1,0:T(8,128)(2,1)}), bf16[128,2048]{1,0:T(8,128)(2,1)}) %all-reduce.3.cloned.1.call-update) | async-done | bytes 524304 | tf_op jit(solution)/shard_map/psum | solution.py:65
  73.6 1.4 fusion.30
  75.0 1.4 multiply_reduce_fusion
  76.4 0.3 multiply_convert_fusion.1
  76.7 0.7 convolution_convert_fusion
  77.4 0.0 copy-start.14
  77.4 27.3 %all_to_all.8 = bf16[4,128,2048]{2,1,0:T(8,128)(2,1)S(1)} all-to-all(bf16[4,128,2048]{2,1,0:T(8,128)(2,1)S(1)} %bitcast.100), channel_id=1, replica_groups=mesh['ep'=4,'tp'=8] {'ep'}, dimensions={0} | all-to-all | bytes 4194304 | tf_op jit(solution)/shard_map/all_to_all | solution.py:88
  104.7 1.3 copy-done.3
  106.0 3.6 %fusion.4 = f32[512,896]{1,0:T(8,128)} fusion(bf16[512,2048]{1,0:T(8,128)(2,1)S(1)} %bitcast.101, bf16[1,2048,896]{2,1,0:T(8,128)(2,1)S(1)} %copy-done.14), kind=kOutput, calls=%fused_computation.4 | convolution fusion | flops 1879048192 | bytes 7602176 | tf_op jit(solution)/shard_map/erd,edf->erf/dot_general | solution.py:91
  109.6 10.2 %fusion.9 = bf16[1,512,2048]{2,1,0:T(8,128)(2,1)} fusion(bf16[1,896,2048]{2,1,0:T(8,128)(2,1)} %param.34, f32[512,896]{1,0:T(8,128)} %fusion.4, bf16[512,2048]{1,0:T(8,128)(2,1)} %bitcast.102, bf16[1,2048,896]{2,1,0:T(8,128)(2,1)} %param.33), kind=kOutput, calls=%fused_computation.8 | convolution fusion | flops 3761897472 | bytes 13369344 | tf_op jit(solution)/shard_map/erf,efd->erd/dot_general | solution.py:94
  119.8 0.0 reduce-scatter.3.cloned.1.call-update
  119.8 0.0 reduce-scatter.5.cloned.1.call-start
  119.9 1.6 fusion.73
  121.5 0.0 copy-start.11
  121.5 0.0 copy-start.6
  121.5 2.8 %convolution_convert_fusion.1 = bf16[128,2048]{1,0:T(8,128)(2,1)} fusion(bf16[256,2048]{1,0:T(8,128)(2,1)S(1)} %copy-done.5, bf16[128,2048]{1,0:T(8,128)(2,1)S(1)} %multiply_convert_fusion.1, bf16[2048,256]{1,0:T(8,128)(2,1)} %param.38, f32[128,256]{1,0:T(8,128)S(1)} %fusion.73), kind=kOutput, calls=%fused_computation.9 | convolution fusion | flops 268894208 | bytes 3276800 | tf_op jit(solution)/shard_map/dot_general | solution.py:109
  124.4 0.0 reduce-scatter.5.cloned.1.call-update
  124.4 0.0 copy-start.16
  124.4 0.7 fusion.38
  125.1 29.4 %reduce-scatter.3.cloned.1.call-done = bf16[1,512,256]{2,1,0:T(8,128)(2,1)} async-done(((bf16[1,512,2048]{2,1,0:T(8,128)(2,1)}), bf16[1,512,256]{2,1,0:T(8,128)(2,1)}) %reduce-scatter.3.cloned.1.call-update) | async-done | bytes 262160 | tf_op jit(solution)/shard_map/reduce_scatter | solution.py:97
  154.6 1.4 copy.120
  155.9 0.5 broadcast.115
  156.4 2.2 %reduce.1 = bf16[512,256]{1,0:T(8,128)(2,1)S(1)} reduce(bf16[512,1,256]{2,1,0:T(2,128)(2,1)S(1)} %bitcast.103, bf16[]{:T(256)} %broadcast.115), dimensions={1}, to_apply=%bitcast.99.reduce_sub_computation | reduce | bytes 524290
  158.7 0.8 reshape.150
  159.4 3.7 %all-to-all-start.1 = ((bf16[4,2,16384]{2,1,0:T(2,128)(2,1)}), bf16[4,2,16384]{2,1,0:T(2,128)(2,1)S(1)}, u32[]{:S(2)}, u32[]{:S(2)}) async-start(bf16[4,2,16384]{2,1,0:T(2,128)(2,1)} %reshape.150), calls=%async_computation.2 | async-start | bytes 524288 | tf_op jit(solution)/shard_map/all_to_all | solution.py:100
  163.1 0.2 fusion.27
  163.3 5.1 %all-to-all-done.1 = bf16[4,2,16384]{2,1,0:T(2,128)(2,1)S(1)} async-done(((bf16[4,2,16384]{2,1,0:T(2,128)(2,1)}), bf16[4,2,16384]{2,1,0:T(2,128)(2,1)S(1)}, u32[]{:S(2)}, u32[]{:S(2)}) %all-to-all-start.1) | async-done | bytes 262176 | tf_op jit(solution)/shard_map/all_to_all | solution.py:100
  168.4 0.3 reshape.151
  168.7 0.3 fusion.14
  169.0 17.6 %reduce-scatter.5.cloned.1.call-done = bf16[128,256]{1,0:T(8,128)(2,1)} async-done(((bf16[128,2048]{1,0:T(8,128)(2,1)}), bf16[128,256]{1,0:T(8,128)(2,1)}) %reduce-scatter.5.cloned.1.call-update) | async-done | bytes 65552 | tf_op jit(solution)/shard_map/reduce_scatter | solution.py:110
  186.7 1.0 fusion.72
  187.7 13.7 %all-reduce = (f32[128]{0:T(128)S(1)}, f32[128]{0:T(128)S(1)}) all-reduce(f32[128]{0:T(128)S(1)} %get-tuple-element.4, f32[128]{0:T(128)S(1)} %get-tuple-element.3), channel_id=1, replica_groups=mesh['ep'=4,'tp'=8] {'tp'}, use_global_device_ids=true, to_apply=%region_14.15 | all-reduce | flops 256 | bytes 2048 | tf_op jit(solution)/shard_map/psum | solution.py:115
  201.4 0.7 multiply_convert_fusion.2
  (31 shorter events, 0.2 us)
Async XLA Ops:
  7.2 5.4 %copy-start = (bf16[256,2048]{1,0:T(8,128)(2,1)S(1)}, bf16[256,2048]{1,0:T(8,128)(2,1)}, u32[]{:S(2)}) copy-start(bf16[256,2048]{1,0:T(8,128)(2,1)} %param.30) | copy-start | bytes 3145732
  7.2 4.8 %copy-start.15 = (bf16[2,128,128]{2,1,0:T(8,128)(2,1)S(1)}, bf16[2,128,128]{2,1,0:T(8,128)(2,1)}, u32[]{:S(2)}) copy-start(bf16[2,128,128]{2,1,0:T(8,128)(2,1)} %param.28) | copy-start | bytes 196612
  7.2 5.2 %copy-start.13 = (f32[256]{0:T(256)S(1)}, f32[256]{0:T(256)}, u32[]{:S(2)}) copy-start(f32[256]{0:T(256)} %param.29) | copy-start | bytes 3076
  7.2 5.2 %copy-start.8 = (f32[128,256]{1,0:T(8,128)S(1)}, f32[128,256]{1,0:T(8,128)}, u32[]{:S(2)}) copy-start(f32[128,256]{1,0:T(8,128)} %param.23) | copy-start | bytes 393220
  7.2 66.4 %all-reduce.3.cloned.1.call-start = ((), (), s32[]{:S(2)}) async-start(), calls=%async_computation.4 | async-start | bytes 1048576 | tf_op jit(solution)/shard_map/psum | solution.py:65
  8.0 4.5 %copy-start.1 = (bf16[128,2048]{1,0:T(8,128)(2,1)S(1)}, bf16[128,2048]{1,0:T(8,128)(2,1)}, u32[]{:S(2)}) copy-start(bf16[128,2048]{1,0:T(8,128)(2,1)} %param.21) | copy-start | bytes 1572868
  8.0 4.5 %copy-start.4 = (bf16[2048,256]{1,0:T(8,128)(2,1)S(1)}, bf16[2048,256]{1,0:T(8,128)(2,1)}, u32[]{:S(2)}) copy-start(bf16[2048,256]{1,0:T(8,128)(2,1)} %param.24) | copy-start | bytes 3145732
  12.4 1.9 copy-start.10
  12.6 4.0 %copy-start.7 = (f32[128,256]{1,0:T(8,128)}, f32[128,256]{1,0:T(8,128)S(1)}, u32[]{:S(2)}) copy-start(f32[128,256]{1,0:T(8,128)S(1)} %multiply_add_fusion.1) | copy-start | bytes 393220
  14.2 62.2 %copy-start.9 = (f32[2048]{0:T(1024)S(1)}, f32[2048]{0:T(1024)}, u32[]{:S(2)}) copy-start(f32[2048]{0:T(1024)} %param.31) | copy-start | bytes 24580
  14.2 140.3 %reduce-scatter.3.cloned.1.call-start = ((), (), s32[]{:S(2)}) async-start(), calls=%async_computation.5 | async-start | bytes 2359296 | tf_op jit(solution)/shard_map/reduce_scatter | solution.py:97
  73.6 2.8 %copy-start.2 = (bf16[128,2048]{1,0:T(8,128)(2,1)S(1)}, bf16[128,2048]{1,0:T(8,128)(2,1)}, u32[]{:S(2)}) copy-start(bf16[128,2048]{1,0:T(8,128)(2,1)} %all-reduce.3.cloned.1.call-done) | copy-start | bytes 1572868
  77.4 28.6 %copy-start.14 = (bf16[1,2048,896]{2,1,0:T(8,128)(2,1)S(1)}, bf16[1,2048,896]{2,1,0:T(8,128)(2,1)}, u32[]{:S(2)}) copy-start(bf16[1,2048,896]{2,1,0:T(8,128)(2,1)} %param.32) | copy-start | bytes 11010052
  104.7 1.3 copy-start.3
  119.8 1.7 copy-start.5
  119.8 66.8 %reduce-scatter.5.cloned.1.call-start = ((), (), s32[]{:S(2)}) async-start(), calls=%async_computation.6 | async-start | bytes 589824 | tf_op jit(solution)/shard_map/reduce_scatter | solution.py:110
  121.5 2.9 %copy-start.11 = (bf16[2048]{0:T(1024)(128)(2,1)S(1)}, bf16[2048]{0:T(1024)(128)(2,1)}, u32[]{:S(2)}) copy-start(bf16[2048]{0:T(1024)(128)(2,1)} %param.40) | copy-start | bytes 12292
  121.5 2.9 %copy-start.6 = (bf16[128,3,256]{2,0,1:T(8,128)(2,1)S(1)}, bf16[128,3,256]{2,0,1:T(8,128)(2,1)}, u32[]{:S(2)}) copy-start(bf16[128,3,256]{2,0,1:T(8,128)(2,1)} %param.22) | copy-start | bytes 589828
  124.4 44.3 %copy-start.16 = (f32[128,2]{0,1:T(2,128)S(1)}, f32[128,2]{0,1:T(2,128)}, u32[]{:S(2)}) copy-start(f32[128,2]{0,1:T(2,128)} %param.36) | copy-start | bytes 3076
  156.4 45.0 %copy-start.12 = (f32[256]{0:T(256)S(1)}, f32[256]{0:T(256)}, u32[]{:S(2)}) copy-start(f32[256]{0:T(256)} %param.41) | copy-start | bytes 3076
  159.4 9.0 %all-to-all-start.1 = ((bf16[4,2,16384]{2,1,0:T(2,128)(2,1)}), bf16[4,2,16384]{2,1,0:T(2,128)(2,1)S(1)}, u32[]{:S(2)}, u32[]{:S(2)}) async-start(bf16[4,2,16384]{2,1,0:T(2,128)(2,1)} %reshape.150), calls=%async_computation.2 | async-start | bytes 524288 | tf_op jit(solution)/shard_map/all_to_all | solution.py:100
Sparse Core Ops, SparseCore 0:
  14.3 59.2 all-reduce.2
  119.9 34.5 reduce-scatter.2
  156.8 29.8 reduce-scatter.4
where the time goes:
time: 209 us
  waiting for transfers between devices  109 us (52%)
  blocking collectives  41 us (20%)
  matrix products  24.2 us (12%)
  between operations  14.1 us (7%)
  other arithmetic  11.1 us (5%)
  local copies, waits for them, and re-layouts  5.33 us (3%)
  starting transfers between devices  3.79 us (2%)
    psum x1, waiting for transfers between devices, on_device(): mixed = lax.psum(partial_mix.astype(jnp.bfloat16), 'tp').astype(jnp.float32)  56.9 us
    reduce_scatter x1, waiting for transfers between devices, on_device(): lax.psum_scatter(partial_out.astype(jnp.bfloat16), 'tp', scatter_dimensio...  29.4 us
    all_to_all x1, blocking collectives, on_device(): lax.all_to_all(dispatch.reshape(experts, capacity, D), 'ep', split_axis=0...  27.3 us
    reduce_scatter x1, waiting for transfers between devices, on_device(): lax.psum_scatter(dense_part.astype(jnp.bfloat16), 'tp', scatter_dimension...  17.6 us
    psum x1, blocking collectives, on_device(): lax.psum((jnp.sum(combined, axis=1), jnp.sum(combined * combined, axis=1)...  13.7 us
    dot_general x1, matrix products, on_device(): jnp.einsum('erf,efd->erd', hidden, expert_down, preferred_element_type=jn...  10.2 us
    all_to_all x1, waiting for transfers between devices, on_device(): lax.all_to_all(reduced, 'ep', split_axis=1, concat_axis=0, tiled=True)  5.13 us
  transfers between devices with their start and end apart: 4, of which 4 were waited for; matrix products, arithmetic and copies ran while one was open for 6% of the time, Pallas kernels for 0%

commit v1 on v0

--- a/solution.py
+++ b/solution.py
@@ -62,7 +62,9 @@
         jnp.bfloat16
     )
     partial_mix = jnp.dot(mixed_rows, out_proj, preferred_element_type=jnp.float32)
-    mixed = lax.psum(partial_mix.astype(jnp.bfloat16), "tp").astype(jnp.float32)
+    mixed = jnp.sum(lax.all_gather(partial_mix.astype(jnp.bfloat16), "tp"), axis=0).astype(
+        jnp.float32
+    )
     normed = norm_rows(ALPHA * tokens.astype(jnp.float32) + mixed, first_gain).astype(jnp.bfloat16)
     tp_index = lax.axis_index("tp")
     tp_count = lax.axis_size("tp")

time: 209 us -> 202 us (0.967)
  waiting for transfers between devices: 109 us -> 98.3 us
  blocking collectives: 41 us -> 43.2 us
    psum x1 -> x0, waiting for transfers between devices: 56.9 us -> none  [on_device(): mixed = lax.psum(partial_mix.astype(jnp.bfloat16), 'tp').astype(jnp.float32)]
    all_gather x0 -> x1, waiting for transfers between devices: none -> 47.3 us  [on_device(): lax.all_gather(partial_mix.astype(jnp.bfloat16), 'tp')]
    reduce_sum x0 -> x1, other arithmetic: none -> 2.95 us  [on_device(): jnp.sum(lax.all_gather(partial_mix.astype(jnp.bfloat16), 'tp'), axis=0)]
    all_to_all x1, blocking collectives: 27.3 us -> 29.5 us  [on_device(): lax.all_to_all(dispatch.reshape(experts, capacity, D), 'ep', split_axis=0...]
  transfers between devices with their start and end apart: 4 -> 4, of which waited for: 4 -> 4; matrix products, arithmetic and copies ran while one was open for 6% -> 7% of each run, Pallas kernels for 0% -> 0%
where the time goes in v1:
time: 202 us; the launch traced here: 201 us
  waiting for transfers between devices  98.3 us (49%)
  blocking collectives  43.2 us (21%)
  matrix products  24.2 us (12%)
  between operations  14.1 us (7%)
  other arithmetic  11.9 us (6%)
  local copies, waits for them, and re-layouts  5.42 us (3%)
  starting transfers between devices  3.95 us (2%)
    all_gather x1, waiting for transfers between devices, on_device(): lax.all_gather(partial_mix.astype(jnp.bfloat16), 'tp')  47.3 us
    all_to_all x1, blocking collectives, on_device(): lax.all_to_all(dispatch.reshape(experts, capacity, D), 'ep', split_axis=0...  29.5 us
    reduce_scatter x1, waiting for transfers between devices, on_device(): lax.psum_scatter(partial_out.astype(jnp.bfloat16), 'tp', scatter_dimensio...  28 us
    reduce_scatter x1, waiting for transfers between devices, on_device(): lax.psum_scatter(dense_part.astype(jnp.bfloat16), 'tp', scatter_dimension...  17.8 us
    psum x1, blocking collectives, on_device(): lax.psum((jnp.sum(combined, axis=1), jnp.sum(combined * combined, axis=1)...  13.8 us
    dot_general x1, matrix products, on_device(): jnp.einsum('erf,efd->erd', hidden, expert_down, preferred_element_type=jn...  10.2 us
    all_to_all x1, waiting for transfers between devices, on_device(): lax.all_to_all(reduced, 'ep', split_axis=1, concat_axis=0, tiled=True)  5.13 us
  transfers between devices with their start and end apart: 4, of which 4 were waited for; matrix products, arithmetic and copies ran while one was open for 7% of the time, Pallas kernels for 0%

profile of v1, /device:TPU:0, one launch (start us, length us, event | category | flops | bytes accessed | tf_op | source)
XLA Modules:
  0.0 201.1 jit_solution(11750110382440669874)
XLA Ops:
  7.2 0.0 copy-start
  7.2 0.0 all-gather.3.cloned.1.call-start
  7.3 0.8 convert_element_type.86
  8.0 1.8 fusion.23
  9.8 1.0 multiply_reduce_fusion.1
  10.8 1.1 fusion.20
  11.9 0.1 copy.91
  12.0 0.2 fusion.17
  12.3 0.1 copy.94
  12.4 0.0 copy-start.9
  12.4 0.1 multiply_add_fusion.1
  12.5 0.0 copy-done
  12.6 0.0 copy-done.1
  12.6 0.0 copy-start.6
  12.6 1.6 convolution_convert_fusion.2
  14.2 0.0 all-gather.3.cloned.1.call-update
  14.2 0.0 reduce-scatter.3.cloned.1.call-start
  14.3 0.1 copy.95
  14.4 0.1 eq.65
  14.5 0.1 eq.61
  14.7 1.2 reduce-window.6
  15.9 0.1 slice.12
  16.0 0.1 copy.97
  16.1 0.1 copy.98
  16.2 0.1 add_bitcast_fusion
  16.3 0.1 reduce_sum.94
  16.5 0.1 copy.99
  16.5 0.1 fusion.34
  16.7 47.3 %all-gather.3.cloned.1.call-done = bf16[1024,2048]{1,0:T(8,128)(2,1)} async-done(((bf16[128,2048]{1,0:T(8,128)(2,1)}), bf16[1024,2048]{1,0:T(8,128)(2,1)}) %all-gather.3.cloned.1.call-update) | async-done | bytes 4194320 | tf_op jit(solution)/shard_map/all_gather | solution.py:65
  64.0 3.0 %reduce_sum.90 = bf16[128,2048]{1,0:T(8,128)(2,1)S(1)} reduce(bf16[8,128,2048]{2,1,0:T(8,128)(2,1)} %bitcast.102, bf16[]{:T(256)} %constant.24.clone.1), dimensions={0}, to_apply=%region_1.2 | reduce | flops 1835008 | bytes 4718594 | tf_op jit(solution)/shard_map/reduce_sum | solution.py:65
  66.9 0.0 copy-start.8
  66.9 0.3 fusion.30
  67.2 0.3 multiply_reduce_fusion
  67.5 0.1 copy-done.8
  67.6 0.3 multiply_convert_fusion.1
  67.9 0.7 convolution_convert_fusion
  68.6 0.0 copy-start.13
  68.7 29.5 %all_to_all.8 = bf16[4,128,2048]{2,1,0:T(8,128)(2,1)S(1)} all-to-all(bf16[4,128,2048]{2,1,0:T(8,128)(2,1)S(1)} %bitcast.101), channel_id=1, replica_groups=mesh['ep'=4,'tp'=8] {'ep'}, dimensions={0} | all-to-all | bytes 4194304 | tf_op jit(solution)/shard_map/all_to_all | solution.py:90
  98.1 1.3 copy-done.2
  99.4 3.6 %fusion.4 = f32[512,896]{1,0:T(8,128)} fusion(bf16[512,2048]{1,0:T(8,128)(2,1)S(1)} %bitcast.103, bf16[1,2048,896]{2,1,0:T(8,128)(2,1)S(1)} %copy-done.13), kind=kOutput, calls=%fused_computation.4 | convolution fusion | flops 1879048192 | bytes 7602176 | tf_op jit(solution)/shard_map/erd,edf->erf/dot_general | solution.py:93
  103.0 10.2 %fusion.9 = bf16[1,512,2048]{2,1,0:T(8,128)(2,1)} fusion(bf16[1,896,2048]{2,1,0:T(8,128)(2,1)} %param.34, f32[512,896]{1,0:T(8,128)} %fusion.4, bf16[512,2048]{1,0:T(8,128)(2,1)} %bitcast.104, bf16[1,2048,896]{2,1,0:T(8,128)(2,1)} %param.33), kind=kOutput, calls=%fused_computation.8 | convolution fusion | flops 3761897472 | bytes 13369344 | tf_op jit(solution)/shard_map/erf,efd->erd/dot_general | solution.py:96
  113.2 0.0 reduce-scatter.3.cloned.1.call-update
  113.2 0.2 reduce-scatter.5.cloned.1.call-start
  113.5 1.6 fusion.73
  115.1 0.0 copy-start.10
  115.1 0.0 copy-start.5
  115.1 2.8 %convolution_convert_fusion.1 = bf16[128,2048]{1,0:T(8,128)(2,1)} fusion(bf16[256,2048]{1,0:T(8,128)(2,1)S(1)} %copy-done.4, bf16[128,2048]{1,0:T(8,128)(2,1)S(1)} %multiply_convert_fusion.1, bf16[2048,256]{1,0:T(8,128)(2,1)} %param.38, f32[128,256]{1,0:T(8,128)S(1)} %fusion.73), kind=kOutput, calls=%fused_computation.9 | convolution fusion | flops 268894208 | bytes 3276800 | tf_op jit(solution)/shard_map/dot_general | solution.py:111
  117.9 0.0 reduce-scatter.5.cloned.1.call-update
  118.0 0.0 copy-start.15
  118.0 0.7 fusion.38
  118.7 28.0 %reduce-scatter.3.cloned.1.call-done = bf16[1,512,256]{2,1,0:T(8,128)(2,1)} async-done(((bf16[1,512,2048]{2,1,0:T(8,128)(2,1)}), bf16[1,512,256]{2,1,0:T(8,128)(2,1)}) %reduce-scatter.3.cloned.1.call-update) | async-done | bytes 262160 | tf_op jit(solution)/shard_map/reduce_scatter | solution.py:99
  146.8 1.4 copy.120
  148.1 0.5 broadcast.115
  148.6 2.2 %reduce.2 = bf16[512,256]{1,0:T(8,128)(2,1)S(1)} reduce(bf16[512,1,256]{2,1,0:T(2,128)(2,1)S(1)} %bitcast.105, bf16[]{:T(256)} %broadcast.115), dimensions={1}, to_apply=%bitcast.100.reduce_sub_computation | reduce | bytes 524290
  150.9 0.8 reshape.151
  151.6 3.6 %all-to-all-start.1 = ((bf16[4,2,16384]{2,1,0:T(2,128)(2,1)}), bf16[4,2,16384]{2,1,0:T(2,128)(2,1)S(1)}, u32[]{:S(2)}, u32[]{:S(2)}) async-start(bf16[4,2,16384]{2,1,0:T(2,128)(2,1)} %reshape.151), calls=%async_computation.2 | async-start | bytes 524288 | tf_op jit(solution)/shard_map/all_to_all | solution.py:102
  155.3 0.2 fusion.27
  155.5 5.1 %all-to-all-done.1 = bf16[4,2,16384]{2,1,0:T(2,128)(2,1)S(1)} async-done(((bf16[4,2,16384]{2,1,0:T(2,128)(2,1)}), bf16[4,2,16384]{2,1,0:T(2,128)(2,1)S(1)}, u32[]{:S(2)}, u32[]{:S(2)}) %all-to-all-start.1) | async-done | bytes 262176 | tf_op jit(solution)/shard_map/all_to_all | solution.py:102
  160.6 0.3 reshape.152
  160.9 0.3 fusion.14
  161.2 17.8 %reduce-scatter.5.cloned.1.call-done = bf16[128,256]{1,0:T(8,128)(2,1)} async-done(((bf16[128,2048]{1,0:T(8,128)(2,1)}), bf16[128,256]{1,0:T(8,128)(2,1)}) %reduce-scatter.5.cloned.1.call-update) | async-done | bytes 65552 | tf_op jit(solution)/shard_map/reduce_scatter | solution.py:112
  179.0 1.0 fusion.72
  180.0 13.8 %all-reduce = (f32[128]{0:T(128)S(1)}, f32[128]{0:T(128)S(1)}) all-reduce(f32[128]{0:T(128)S(1)} %get-tuple-element.4, f32[128]{0:T(128)S(1)} %get-tuple-element.3), channel_id=1, replica_groups=mesh['ep'=4,'tp'=8] {'tp'}, use_global_device_ids=true, to_apply=%region_14.15 | all-reduce | flops 256 | bytes 2048 | tf_op jit(solution)/shard_map/psum | solution.py:117
  193.8 0.7 multiply_convert_fusion.2
  (30 shorter events, 0.2 us)
Async XLA Ops:
  7.2 5.4 %copy-start = (bf16[256,2048]{1,0:T(8,128)(2,1)S(1)}, bf16[256,2048]{1,0:T(8,128)(2,1)}, u32[]{:S(2)}) copy-start(bf16[256,2048]{1,0:T(8,128)(2,1)} %param.30) | copy-start | bytes 3145732
  7.2 4.8 %copy-start.14 = (bf16[2,128,128]{2,1,0:T(8,128)(2,1)S(1)}, bf16[2,128,128]{2,1,0:T(8,128)(2,1)}, u32[]{:S(2)}) copy-start(bf16[2,128,128]{2,1,0:T(8,128)(2,1)} %param.28) | copy-start | bytes 196612
  7.2 5.2 %copy-start.12 = (f32[256]{0:T(256)S(1)}, f32[256]{0:T(256)}, u32[]{:S(2)}) copy-start(f32[256]{0:T(256)} %param.29) | copy-start | bytes 3076
  7.2 5.2 %copy-start.7 = (f32[128,256]{1,0:T(8,128)S(1)}, f32[128,256]{1,0:T(8,128)}, u32[]{:S(2)}) copy-start(f32[128,256]{1,0:T(8,128)} %param.23) | copy-start | bytes 393220
  7.2 56.7 %all-gather.3.cloned.1.call-start = ((), (), s32[]{:S(2)}) async-start(), calls=%async_computation.6 | async-start | bytes 4718592 | tf_op jit(solution)/shard_map/all_gather | solution.py:65
  8.0 4.5 %copy-start.1 = (bf16[128,2048]{1,0:T(8,128)(2,1)S(1)}, bf16[128,2048]{1,0:T(8,128)(2,1)}, u32[]{:S(2)}) copy-start(bf16[128,2048]{1,0:T(8,128)(2,1)} %param.21) | copy-start | bytes 1572868
  8.0 4.5 %copy-start.3 = (bf16[2048,256]{1,0:T(8,128)(2,1)S(1)}, bf16[2048,256]{1,0:T(8,128)(2,1)}, u32[]{:S(2)}) copy-start(bf16[2048,256]{1,0:T(8,128)(2,1)} %param.24) | copy-start | bytes 3145732
  12.4 1.9 copy-start.9
  12.6 4.0 %copy-start.6 = (f32[128,256]{1,0:T(8,128)}, f32[128,256]{1,0:T(8,128)S(1)}, u32[]{:S(2)}) copy-start(f32[128,256]{1,0:T(8,128)S(1)} %multiply_add_fusion.1) | copy-start | bytes 393220
  14.2 132.5 %reduce-scatter.3.cloned.1.call-start = ((), (), s32[]{:S(2)}) async-start(), calls=%async_computation.4 | async-start | bytes 2359296 | tf_op jit(solution)/shard_map/reduce_scatter | solution.py:99
  66.9 0.7 copy-start.8
  68.6 30.8 %copy-start.13 = (bf16[1,2048,896]{2,1,0:T(8,128)(2,1)S(1)}, bf16[1,2048,896]{2,1,0:T(8,128)(2,1)}, u32[]{:S(2)}) copy-start(bf16[1,2048,896]{2,1,0:T(8,128)(2,1)} %param.32) | copy-start | bytes 11010052
  98.1 1.3 copy-start.2
  113.2 1.9 copy-start.4
  113.2 65.7 %reduce-scatter.5.cloned.1.call-start = ((), (), s32[]{:S(2)}) async-start(), calls=%async_computation.5 | async-start | bytes 589824 | tf_op jit(solution)/shard_map/reduce_scatter | solution.py:112
  115.1 2.9 %copy-start.10 = (bf16[2048]{0:T(1024)(128)(2,1)S(1)}, bf16[2048]{0:T(1024)(128)(2,1)}, u32[]{:S(2)}) copy-start(bf16[2048]{0:T(1024)(128)(2,1)} %param.40) | copy-start | bytes 12292
  115.1 2.9 %copy-start.5 = (bf16[128,3,256]{2,0,1:T(8,128)(2,1)S(1)}, bf16[128,3,256]{2,0,1:T(8,128)(2,1)}, u32[]{:S(2)}) copy-start(bf16[128,3,256]{2,0,1:T(8,128)(2,1)} %param.22) | copy-start | bytes 589828
  118.0 42.9 %copy-start.15 = (f32[128,2]{0,1:T(2,128)S(1)}, f32[128,2]{0,1:T(2,128)}, u32[]{:S(2)}) copy-start(f32[128,2]{0,1:T(2,128)} %param.36) | copy-start | bytes 3076
  148.6 45.2 %copy-start.11 = (f32[256]{0:T(256)S(1)}, f32[256]{0:T(256)}, u32[]{:S(2)}) copy-start(f32[256]{0:T(256)} %param.41) | copy-start | bytes 3076
  151.6 9.0 %all-to-all-start.1 = ((bf16[4,2,16384]{2,1,0:T(2,128)(2,1)}), bf16[4,2,16384]{2,1,0:T(2,128)(2,1)S(1)}, u32[]{:S(2)}, u32[]{:S(2)}) async-start(bf16[4,2,16384]{2,1,0:T(2,128)(2,1)} %reshape.151), calls=%async_computation.2 | async-start | bytes 524288 | tf_op jit(solution)/shard_map/all_to_all | solution.py:102
Sparse Core Ops, SparseCore 0:
  14.3 49.5 all-gather.2
  113.3 33.3 reduce-scatter.2
  149.0 29.9 reduce-scatter.4
